TPU v7x, 512 devices: a whole 4x4x16 slice. The times are simulated.
512 devices in a mesh: sp: 32 (over z, core), tp: 16 (over y, x).
Axes of the slice: x: 4, y: 4, z: 16, core: 2. Of those that a mesh axis runs over, the one named last changes fastest.
Arguments:
- query_proj: bfloat16 [8192, 2048], P('sp', 'tp'), may hold values from -4 to 4
- key_proj: bfloat16 [8192, 1024], P('sp', 'tp'), may hold values from -4 to 4
- value_proj: bfloat16 [8192, 1024], P('sp', 'tp'), may hold values from -48 to 48
- query_gain: float32 [32, 64], P('tp'), may hold values from 1 to 6
- key_gain: float32 [16, 64], P('tp'), may hold values from 1 to 6
- residual: bfloat16 [8192, 2048], P('sp', 'tp'), may hold values from -48 to 48
- out_weight: bfloat16 [2048, 2048], P(None, 'tp'), may hold values from -0.125 to 0.125
- route_expert: int32 [8192, 8], P('sp'), may hold values from 0 to 255, all different within a row; in each aligned block of 256 rows (0 to 255, 256 to 511, ...) at most 12 rows name the same one
- route_weight: float32 [8192, 8], P('sp'), may hold values from 0.25 to 1.25
- expert_gate: bfloat16 [512, 2048, 256], P(('sp', 'tp')), may hold values from -0.125 to 0.125
- expert_up: bfloat16 [512, 2048, 256], P(('sp', 'tp')), may hold values from -0.125 to 0.125
- expert_down: bfloat16 [512, 256, 2048], P(('sp', 'tp')), may hold values from -0.25 to 0.25
Outputs:
- block_out: bfloat16 [8192, 2048], P('sp', 'tp')
Inputs may be any that keep to these rules, and one draw needn't show every extreme that they name: `route_expert`: A row names 8 different experts; among the rows of one index of sp no expert is named by more than 12 rows, a bound that some block reaches of them.
All inputs are finite; a program needn't handle non-finite values.
Results may differ from a plain program's by a relative error of at most 0.012.
The roundings to bfloat16 on the way count: a program that leaves them out, or rounds other values in their place, can miss the bound.
Values may be sent and summed in bfloat16 or wider, within the bound.
A program may use at most 64 MiB of HBM per device.

v0:
```python
import math

import jax
import jax.numpy as jnp
from jax import lax
from jax.sharding import Mesh
from jax.sharding import PartitionSpec as P

HEAD_DIM = 64
TOP_K = 8
GRID_W = 64
SP = ("sp_0", "sp_1")
SP_TP = ("sp_0", "sp_1", "tp")


EPSILON = 1e-06
ROPE_BASE = 10000.0
KEY_BLOCK = 1024


def laid_out(pieces, dim):
    shape = list(pieces.shape[1:])
    shape[dim] *= pieces.shape[0]
    return jnp.moveaxis(pieces, 0, dim).reshape(shape)


def from_everyone(x, axis):
    devices = lax.axis_size(axis)
    return lax.all_to_all(jnp.broadcast_to(x[None], (devices, *x.shape)), axis, 0, 0, tiled=True)


def gather_directly(x, axis, dim):
    return laid_out(from_everyone(x, axis), dim)


def cut_along(x, dim, devices):
    shape = x.shape
    pieces = x.reshape(*shape[:dim], devices, shape[dim] // devices, *shape[dim + 1 :])
    return jnp.moveaxis(pieces, dim, 0)


def turned_blocks(pieces, axes, sequence):
    shape = [lax.axis_size(a) for a in axes]
    pieces = pieces.reshape(*shape, *pieces.shape[1:])
    for k in sequence:
        pieces = lax.all_to_all(pieces, axes[k], split_axis=k, concat_axis=k, tiled=True)
    return pieces.reshape(-1, *pieces.shape[len(axes) :])


def core_and_chips(x, groups, sequence, split_dim, concat_dim):
    devices = lax.axis_size(groups[0]) * lax.axis_size(groups[1])
    pieces = cut_along(x, split_dim, devices)
    return laid_out(turned_blocks(pieces, groups, sequence), concat_dim)


def swapped(value, axis, stride):
    mask = 2**stride
    pairs = [(source, source ^ mask) for source in range(lax.axis_size(axis))]
    return lax.ppermute(value, axis, pairs)


def summed_on_arrival(x, axis, dim):
    devices = lax.axis_size(axis)
    pieces = lax.all_to_all(cut_along(x, dim, devices), axis, 0, 0, tiled=True)
    return jnp.sum(pieces.astype(jnp.float32), axis=0)


def rotation_tables(offset, count):
    pair_count = HEAD_DIM // 4
    position = offset + jnp.arange(count, dtype=jnp.int32)
    grid_row = (position // GRID_W).astype(jnp.float32)
    grid_col = (position % GRID_W).astype(jnp.float32)
    inverse = ROPE_BASE ** (-jnp.arange(pair_count, dtype=jnp.float32) / pair_count)
    angles = jnp.stack([grid_row[:, None] * inverse, grid_col[:, None] * inverse], axis=1)
    return (jnp.cos(angles), jnp.sin(angles))


def rotate(vectors, cosine_table, sine_table):
    pair_count = HEAD_DIM // 4
    shaped = vectors.reshape(vectors.shape[:-1] + (2, 2, pair_count))
    first_half = shaped[..., 0, :]
    second_half = shaped[..., 1, :]
    cosine_row = cosine_table[:, None]
    sine_row = sine_table[:, None]
    turned = jnp.stack(
        [
            first_half * cosine_row - second_half * sine_row,
            first_half * sine_row + second_half * cosine_row,
        ],
        axis=-2,
    )
    return turned.reshape(vectors.shape)


def head_norm(vectors, gain):
    scaled = vectors.astype(jnp.float32)
    scaled = scaled * lax.rsqrt(jnp.mean(scaled * scaled, axis=-1, keepdims=True) + EPSILON)
    return scaled * gain


def online_update(running, query_groups, key_block, value_block):
    running_max, running_sum, running_acc = running
    scores = jnp.einsum(
        "tkgd,nkd->kgtn", query_groups, key_block, preferred_element_type=jnp.float32
    ) * HEAD_DIM ** (-0.5)
    new_max = jnp.maximum(running_max, jnp.max(scores, axis=-1))
    rescale = jnp.exp(running_max - new_max)
    weights = jnp.exp(scores - new_max[..., None]).astype(jnp.bfloat16)
    new_sum = running_sum * rescale + jnp.sum(weights.astype(jnp.float32), axis=-1)
    update = jnp.einsum("kgtn,nkd->kgtd", weights, value_block, preferred_element_type=jnp.float32)
    return (new_max, new_sum, running_acc * rescale[..., None] + update)


def local(
    query_proj,
    key_proj,
    value_proj,
    query_gain,
    key_gain,
    residual,
    out_weight,
    route_expert,
    route_weight,
    expert_gate,
    expert_up,
    expert_down,
):
    token_count = query_proj.shape[0]
    local_heads = query_gain.shape[0]
    local_kv = key_gain.shape[0]
    group_size = local_heads // local_kv
    sp_size = lax.axis_size(SP)
    tp_size = lax.axis_size("tp")
    tp_place = lax.axis_index("tp")
    offset = lax.axis_index(SP) * token_count
    cosine_table, sine_table = rotation_tables(offset, token_count)
    query_rot = rotate(
        head_norm(query_proj.reshape(token_count, local_heads, HEAD_DIM), query_gain),
        cosine_table,
        sine_table,
    ).astype(jnp.bfloat16)
    key_rot = rotate(
        head_norm(key_proj.reshape(token_count, local_kv, HEAD_DIM), key_gain),
        cosine_table,
        sine_table,
    ).astype(jnp.bfloat16)
    packed = jnp.concatenate(
        [key_rot.reshape(token_count, local_kv * HEAD_DIM), value_proj], axis=1
    )
    query_groups = query_rot.reshape(token_count, local_kv, group_size, HEAD_DIM)
    initial = (
        jnp.full((local_kv, group_size, token_count), -1e30, jnp.float32),
        jnp.zeros((local_kv, group_size, token_count), jnp.float32),
        jnp.zeros((local_kv, group_size, token_count, HEAD_DIM), jnp.float32),
    )
    incoming = lax.all_gather(packed, SP, axis=0, tiled=True)
    incoming_len = incoming.shape[0]
    step_len = math.gcd(incoming_len, KEY_BLOCK)

    def one_step(step_index, running):
        block_rows = lax.dynamic_slice_in_dim(incoming, step_index * step_len, step_len, 0)
        key_block = block_rows[:, : local_kv * HEAD_DIM].reshape(step_len, local_kv, HEAD_DIM)
        value_block = block_rows[:, local_kv * HEAD_DIM :].reshape(step_len, local_kv, HEAD_DIM)
        return online_update(running, query_groups, key_block, value_block)

    final_max, final_sum, final_acc = lax.fori_loop(0, incoming_len // step_len, one_step, initial)
    attended = final_acc / final_sum[..., None]
    attended = jnp.transpose(attended, (2, 0, 1, 3)).reshape(token_count, local_heads * HEAD_DIM)
    attended = attended.astype(jnp.bfloat16)
    projected = jnp.dot(
        gather_directly(attended, "tp", 1), out_weight, preferred_element_type=jnp.float32
    )
    mixed_sum = residual.astype(jnp.float32) + projected
    mixed_rows = mixed_sum.astype(jnp.bfloat16)
    full_rows = gather_directly(mixed_rows, "tp", 1)
    width_total = full_rows.shape[1]
    per_sp = tp_size // 2
    column = tp_place // 2
    half = tp_place % 2
    experts_total = per_sp * sp_size
    capacity = 3 * token_count * TOP_K // (2 * experts_total)
    slot_count = sp_size * capacity
    flat_choice = route_expert.reshape(token_count * TOP_K)
    onehot = (flat_choice[:, None] == jnp.arange(experts_total, dtype=jnp.int32)[None, :]).astype(
        jnp.int32
    )
    earlier = jnp.cumsum(onehot, axis=0) - onehot
    slot_rank = jnp.sum(earlier * onehot, axis=1)
    mine = flat_choice % per_sp == column
    target = flat_choice // per_sp * capacity + slot_rank
    owner = jnp.arange(token_count * TOP_K, dtype=jnp.int32) // TOP_K
    slot_token = (
        jnp.full((slot_count + 1,), token_count, jnp.int32)
        .at[jnp.where(mine, target, slot_count)]
        .set(owner)[:slot_count]
    )
    padded = jnp.concatenate([full_rows, jnp.zeros((1, width_total), jnp.bfloat16)], axis=0)
    selected = padded[slot_token].reshape(sp_size, capacity, width_total)
    half_cap = capacity // 2
    own_part = lax.dynamic_slice_in_dim(selected, half * half_cap, half_cap, 1)
    received = core_and_chips(own_part, ("sp_0", "sp_1"), (1, 0), 0, 0)
    partner = swapped(received, "tp", 0)
    arrived = jnp.where(
        half == 0,
        jnp.concatenate([received, partner], axis=1),
        jnp.concatenate([partner, received], axis=1),
    )
    expert_rows = arrived.reshape(slot_count, width_total)
    squares = jnp.mean(jnp.square(expert_rows.astype(jnp.float32)), axis=-1, keepdims=True)
    norm_scale = lax.rsqrt(squares + EPSILON)
    gate_value = (
        jnp.dot(expert_rows, expert_gate[0], preferred_element_type=jnp.float32) * norm_scale
    )
    up_value = jnp.dot(expert_rows, expert_up[0], preferred_element_type=jnp.float32) * norm_scale
    hidden = (jax.nn.silu(gate_value) * up_value).astype(jnp.bfloat16)
    half_result = jnp.dot(hidden, expert_down[0], preferred_element_type=jnp.float32).astype(
        jnp.bfloat16
    )
    returned = core_and_chips(
        half_result.reshape(sp_size, capacity, width_total), ("sp_0", "sp_1"), (1, 0), 0, 0
    )
    slot_results = returned.reshape(slot_count, width_total)
    mine_grid = mine.reshape(token_count, TOP_K)
    target_grid = target.reshape(token_count, TOP_K)
    gathered_sum = jnp.zeros((token_count, width_total), jnp.float32)
    for choice_index in range(TOP_K):
        chosen = mine_grid[:, choice_index]
        index = jnp.where(chosen, target_grid[:, choice_index], 0)
        factor = jnp.where(chosen, route_weight[:, choice_index], 0.0)
        picked = slot_results[index].astype(jnp.float32)
        gathered_sum = gathered_sum + factor[:, None] * picked
    routed = summed_on_arrival(gathered_sum.astype(jnp.bfloat16), "tp", 1)
    return (mixed_sum + routed).astype(jnp.bfloat16)


def solution(mesh):
    split = Mesh(mesh.devices.reshape(16, 2, mesh.shape["tp"]), ("sp_0", "sp_1", "tp"))
    in_specs = (
        P(SP, "tp"),
        P(SP, "tp"),
        P(SP, "tp"),
        P("tp", None),
        P("tp", None),
        P(SP, "tp"),
        P(None, "tp"),
        P(SP, None),
        P(SP, None),
        P(SP_TP, None, None),
        P(SP_TP, None, None),
        P(SP_TP, None, None),
    )
    out_specs = P(SP, "tp")
    return jax.shard_map(local, mesh=split, in_specs=in_specs, out_specs=out_specs, check_vma=False)
```

profile of v0, /device:TPU:1, one launch (start us, length us, event | category | flops | bytes accessed | tf_op | source)
XLA Modules:
  0.0 395.4 jit_solution(6346549353143653187)
XLA Ops:
  13.3 75.3 %all-gather.2.cloned.1.call-done = bf16[8192,128]{0,1:T(8,128)(2,1)} async-done(((bf16[256,128]{0,1:T(8,128)(2,1)}), bf16[8192,128]{0,1:T(8,128)(2,1)}) %all-gather.2.cloned.1.call-update) | async-done | bytes 2097168 | tf_op jit(solution)/shard_map/all_gather | solution.py:156
  88.6 25.7 %while.18 = (s32[]{:T(128)}, f32[1,2,256]{2,1,0:T(2,128)S(1)}, f32[1,2,256]{2,1,0:T(2,128)S(1)}, f32[1,2,256,64]{2,3,1,0:T(8,128)S(1)}, bf16[8192,128]{0,1:T(8,1...) while((s32[]{:T(128)}, f32[1,2,256]{2,1,0:T(2,128)S(1)}, ...), condition=%wide.region_5.6_spmd.clone, body=%wide.region_2.5_spmd.clone.sunk | while | flops 139561984 | bytes 6914247 | solution.py:166
  115.5 6.6 %all-to-all-start = ((bf16[16,256,128]{1,2,0:T(8,128)(2,1)}), bf16[16,256,128]{1,2,0:T(8,128)(2,1)}, u32[]{:S(2)}, u32[]{:S(2)}) async-start(bf16[16,256,128]{1,2,0:T(8,128)(2,1)} %broadcast_in_dim.47), calls=%async_computation | async-start | bytes 2097152 | tf_op jit(solution)/shard_map/all_to_all | solution.py:29
  124.0 14.6 %all-to-all-done = bf16[16,256,128]{1,2,0:T(8,128)(2,1)} async-done(((bf16[16,256,128]{1,2,0:T(8,128)(2,1)}), bf16[16,256,128]{1,2,0:T(8,128)(2,1)}, u32[]{:S(2)}, u32[]{:S(2)}) %all-to-all-start) | async-done | bytes 1048608 | tf_op jit(solution)/shard_map/all_to_all | solution.py:29
  141.7 4.5 %all-to-all-start.1 = ((bf16[16,256,128]{2,1,0:T(8,128)(2,1)}), bf16[16,256,128]{2,1,0:T(8,128)(2,1)}, u32[]{:S(2)}, u32[]{:S(2)}) async-start(bf16[16,256,128]{2,1,0:T(8,128)(2,1)} %broadcast_in_dim.49), calls=%async_computation.1 | async-start | bytes 2097152 | tf_op jit(solution)/shard_map/all_to_all | solution.py:29
  147.2 8.0 %scatter_custom_fusion = s32[385]{0:T(512)S(1)} fusion(s32[2048]{0:T(1024)S(1)} %bitcast.222, s32[2048]{0:T(1024)S(1)} %add_select_fusion.2, s32[]{:T(128)} %constant.176.clone.1), kind=kCustom, calls=%fused_computation.181 | custom fusion | bytes 1544 | tf_op jit(solution)/shard_map/scatter | solution.py:195
  155.3 6.2 %all-to-all-done.1 = bf16[16,256,128]{2,1,0:T(8,128)(2,1)} async-done(((bf16[16,256,128]{2,1,0:T(8,128)(2,1)}), bf16[16,256,128]{2,1,0:T(8,128)(2,1)}, u32[]{:S(2)}, u32[]{:S(2)}) %all-to-all-start.1) | async-done | bytes 1048608 | tf_op jit(solution)/shard_map/all_to_all | solution.py:29
  163.0 3.1 gather_fusion
  166.1 2.4 reshape.662
  169.4 7.1 %all_to_all.35 = bf16[16,2,1,6,2048]{4,0,3,2,1:T(8,128)(2,1)S(1)} all-to-all(bf16[16,2,1,6,2048]{4,0,3,2,1:T(8,128)(2,1)S(1)} %copy.136), channel_id=1, replica_groups=mesh['sp_0'=16,'sp_1'=2,'tp'=16] {'sp_1'}, dimensions={1} | all-to-all | bytes 1572864 | tf_op jit(solution)/shard_map/all_to_all | solution.py:46
  177.3 42.1 %all_to_all.36 = bf16[16,2,1,6,2048]{4,1,3,2,0:T(2,128)(2,1)S(1)} all-to-all(bf16[16,2,1,6,2048]{4,1,3,2,0:T(2,128)(2,1)S(1)} %copy.137), channel_id=1, replica_groups=mesh['sp_0'=16,'sp_1'=2,'tp'=16] {'sp_0'}, dimensions={0} | all-to-all | bytes 1572864 | tf_op jit(solution)/shard_map/all_to_all | solution.py:46
  222.4 12.4 %collective-permute-done = bf16[32,6,2048]{2,0,1:T(8,128)(2,1)S(1)} collective-permute-done((bf16[32,6,2048]{2,0,1:T(8,128)(2,1)S(1)}, bf16[32,6,2048]{2,0,1:T(8,128)(2,1)S(1)}, u32[]{:S(2)}, u32[]{:S(2)}) %collective-permute-start) | collective-permute-done | bytes 786464 | tf_op jit(solution)/shard_map/ppermute | solution.py:59
  240.6 2.4 convolution_multiply_fusion
  243.1 4.2 %convolution_convert_fusion = bf16[384,2048]{1,0:T(8,128)(2,1)} fusion(bf16[1,256,2048]{2,1,0:T(8,128)(2,1)S(1)} %copy-done, f32[384,256]{1,0:T(8,128)S(1)} %convolution_multiply_fusion, bf16[384,2048]{1,0:T(8,128)(2,1)S(1)} %copy-done.1, bf16[1,2048,256]{2,1,0:T(8,128)(2,1)} %param.23, f32[384]{0:T(512)S(1)} %rsqrt.30), kind=kOutput, calls=%fused_computation.32 | convolution fusion | flops 806780928 | bytes 5637632 | tf_op jit(solution)/shard_map/dot_general | solution.py:216
  247.3 2.4 reshape_reshape_reshape.6
  250.5 11.9 %all_to_all.37 = bf16[16,2,1,12,2048]{4,0,3,2,1:T(8,128)(2,1)S(1)} all-to-all(bf16[16,2,1,12,2048]{4,0,3,2,1:T(8,128)(2,1)S(1)} %copy.141), channel_id=1, replica_groups=mesh['sp_0'=16,'sp_1'=2,'tp'=16] {'sp_1'}, dimensions={1} | all-to-all | bytes 3145728 | tf_op jit(solution)/shard_map/all_to_all | solution.py:46
  262.4 2.8 copy.142
  265.2 11.2 %all-to-all-start.5 = ((bf16[16,2,1,12,2048]{4,1,3,2,0:T(2,128)(2,1)}), bf16[16,2,1,12,2048]{4,1,3,2,0:T(2,128)(2,1)S(1)}, u32[]{:S(2)}, u32[]{:S(2)}) async-start(bf16[16,2,1,12,2048]{4,1,3,2,0:T(2,128)(2,1)} %copy.142), calls=%async_computation.5 | async-start | bytes 3145728 | tf_op jit(solution)/shard_map/all_to_all | solution.py:46
  283.9 61.6 %all-to-all-done.5 = bf16[16,2,1,12,2048]{4,1,3,2,0:T(2,128)(2,1)S(1)} async-done(((bf16[16,2,1,12,2048]{4,1,3,2,0:T(2,128)(2,1)}), bf16[16,2,1,12,2048]{4,1,3,2,0:T(2,128)(2,1)S(1)}, u32[]{:S(2)}, u32[]{:S(2)}) %all-to-all-start.5) | async-done | bytes 1572896 | tf_op jit(solution)/shard_map/all_to_all | solution.py:46
  347.5 2.5 reshape_reshape_reshape.7
  354.7 2.4 gather_fusion.6
  364.1 2.4 gather_fusion.2
  368.8 4.4 %fusion.26 = bf16[16,256,128]{2,1,0:T(8,128)(2,1)S(1)} fusion(f32[256]{0:T(256)S(1)} %get-tuple-element.147, f32[256]{0:T(256)S(1)} %get-tuple-element.148, f32[256]{0:T(256)S(1)} %get-tuple-element.149, f32[256]{0:T(256)S(1)} %get-tuple-element.150, f32[256]{0:T(256)S(1)} %get-tuple-element.151, f32[256]{0:T(256)S(1)} %get-tuple-element.152, ...), kind=kLoop, calls=%fused_computation.75 | loop fusion | flops 12582912 | bytes 9445376 | tf_op jit(solution)/shard_map/transpose | solution.py:39
  373.2 14.6 %all_to_all.38 = bf16[16,256,128]{2,1,0:T(8,128)(2,1)S(1)} all-to-all(bf16[16,256,128]{2,1,0:T(8,128)(2,1)S(1)} %fusion.26), channel_id=1, replica_groups=mesh['sp_0'=16,'sp_1'=2,'tp'=16] {'tp'}, dimensions={0} | all-to-all | bytes 2097152 | tf_op jit(solution)/shard_map/all_to_all | solution.py:64
  (140 shorter events, 76.1 us)
Async XLA Ops:
  6.5 236.5 %copy-start = (bf16[1,256,2048]{2,1,0:T(8,128)(2,1)S(1)}, bf16[1,256,2048]{2,1,0:T(8,128)(2,1)}, u32[]{:S(2)}) copy-start(bf16[1,256,2048]{2,1,0:T(8,128)(2,1)} %param.25) | copy-start | bytes 3145732
  6.5 82.1 %all-gather.2.cloned.1.call-start = ((), (), s32[]{:S(2)}) async-start(), calls=%async_computation.7 | async-start | bytes 2162688 | tf_op jit(solution)/shard_map/all_gather | solution.py:156
  115.5 23.1 %all-to-all-start = ((bf16[16,256,128]{1,2,0:T(8,128)(2,1)}), bf16[16,256,128]{1,2,0:T(8,128)(2,1)}, u32[]{:S(2)}, u32[]{:S(2)}) async-start(bf16[16,256,128]{1,2,0:T(8,128)(2,1)} %broadcast_in_dim.47), calls=%async_computation | async-start | bytes 2097152 | tf_op jit(solution)/shard_map/all_to_all | solution.py:29
  122.7 15.9 %copy-start.2 = (bf16[256,128]{1,0:T(8,128)(2,1)S(1)}, bf16[256,128]{1,0:T(8,128)(2,1)}, u32[]{:S(2)}) copy-start(bf16[256,128]{1,0:T(8,128)(2,1)} %param.19) | copy-start | bytes 196612
  141.7 19.9 %all-to-all-start.1 = ((bf16[16,256,128]{2,1,0:T(8,128)(2,1)}), bf16[16,256,128]{2,1,0:T(8,128)(2,1)}, u32[]{:S(2)}, u32[]{:S(2)}) async-start(bf16[16,256,128]{2,1,0:T(8,128)(2,1)} %broadcast_in_dim.49), calls=%async_computation.1 | async-start | bytes 2097152 | tf_op jit(solution)/shard_map/all_to_all | solution.py:29
  220.3 14.6 %collective-permute-start = (bf16[32,6,2048]{2,0,1:T(8,128)(2,1)S(1)}, bf16[32,6,2048]{2,0,1:T(8,128)(2,1)S(1)}, u32[]{:S(2)}, u32[]{:S(2)}) collective-permute-start(bf16[32,6,2048]{2,0,1:T(8,128)(2,1)S(1)} %reshape_reshape.7), channel_id=1, source_target_pairs={{0,1},{1,0},{2,3},{3,2},{4,5},{5,4},{6,7},{7,6},{8,9},{9,8},{10,11... | collective-permute-start | bytes 2359304 | tf_op jit(solution)/shard_map/ppermute | solution.py:59
  240.6 2.4 copy-start.1
  265.2 11.9 %copy-start.3 = (f32[256,8]{0,1:T(8,128)S(1)}, f32[256,8]{0,1:T(8,128)}, u32[]{:S(2)}) copy-start(f32[256,8]{0,1:T(8,128)} %param.22) | copy-start | bytes 24580
  265.2 80.2 %all-to-all-start.5 = ((bf16[16,2,1,12,2048]{4,1,3,2,0:T(2,128)(2,1)}), bf16[16,2,1,12,2048]{4,1,3,2,0:T(2,128)(2,1)S(1)}, u32[]{:S(2)}, u32[]{:S(2)}) async-start(bf16[16,2,1,12,2048]{4,1,3,2,0:T(2,128)(2,1)} %copy.142), calls=%async_computation.5 | async-start | bytes 3145728 | tf_op jit(solution)/shard_map/all_to_all | solution.py:46
Sparse Core Ops, SparseCore 0:
  10.1 78.5 all-gather.1
where the time goes:
time: 402 us; the launch traced here: 395 us
  waiting for transfers between devices  170 us (42%)
  blocking collectives  75.7 us (19%)
  local copies, waits for them, and re-layouts  61.2 us (15%)
  matrix products  30.6 us (8%)
  starting transfers between devices  24.4 us (6%)
  other arithmetic  19.1 us (5%)
  between operations  13.9 us (3%)
    all_gather x1, waiting for transfers between devices, local(): incoming = lax.all_gather(packed, SP, axis=0, tiled=True)  75.3 us
    all_to_all x1, waiting for transfers between devices, turned_blocks(): lax.all_to_all(pieces, axes[k], split_axis=k, concat_axis=k, tiled=True)  61.6 us
    all_to_all x3, blocking collectives, turned_blocks(): lax.all_to_all(pieces, axes[k], split_axis=k, concat_axis=k, tiled=True)  61.1 us
    all_to_all x2, waiting for transfers between devices, from_everyone(): lax.all_to_all(jnp.broadcast_to(x[None], (devices, *x.shape)), axis, 0, 0...  20.8 us
    gather x8, local copies, waits for them, and re-layouts, local(): picked = slot_results[index].astype(jnp.float32)  18.8 us
    all_to_all x1, blocking collectives, summed_on_arrival(): pieces = lax.all_to_all(cut_along(x, dim, devices), axis, 0, 0, tiled=True)  14.6 us
    ppermute x1, waiting for transfers between devices, swapped(): return lax.ppermute(value, axis, pairs)  12.4 us
    all_to_all x1, starting transfers between devices, turned_blocks(): lax.all_to_all(pieces, axes[k], split_axis=k, concat_axis=k, tiled=True)  11.2 us
  transfers between devices with their start and end apart: 5, of which 5 were waited for; matrix products, arithmetic and copies ran while one was open for 5% of the time, Pallas kernels for 0%

commit v1 on v0

v1 whole, which is shorter than its diff:
```python
import functools

import jax
import jax.numpy as jnp
import numpy as np
from jax import lax
from jax.experimental import pallas as pl
from jax.experimental.pallas import tpu as pltpu
from jax.sharding import Mesh
from jax.sharding import PartitionSpec as P

EPS = 1e-06
CAP = 12
TOK = 256
HALF = 128
LANES = 128
GROUP = 4 * CAP
F32 = jnp.float32
BF16 = jnp.bfloat16
MESH = pl.DeviceIdType.MESH
SP = ("z", "c")
TP = ("y", "x")
ALL = ("z", "c", "y", "x")


def rotation_constants(rows):
    pairs = 16
    inverse = np.float32(10000.0) ** (-np.arange(pairs, dtype=np.float32) / np.float32(pairs))
    inverse = inverse.astype(np.float32)
    lane = np.arange(LANES)
    freq = inverse[lane % 16]
    sign = np.where((lane // 16) % 2 == 0, -1.0, 1.0)

    def table(count):
        angle = (np.arange(count, dtype=np.float32)[:, None] * freq[None, :]).astype(np.float32)
        angle = angle.astype(np.float64)
        return np.stack([np.cos(angle), np.sin(angle) * sign[None, :]]).astype(np.float32)

    return table(rows), table(64)


def places():
    return lax.axis_index("z"), lax.axis_index("c"), lax.axis_index("y"), lax.axis_index("x")


def plane_id(place, nx):
    return {"y": place // nx, "x": place % nx}


def barrier_all(z, c, me, nz, ntp, nx):
    barrier = pltpu.get_barrier_semaphore()

    def one(d, carry):
        t = (me + d) % ntp
        pl.semaphore_signal(barrier, inc=1, device_id=plane_id(t, nx), device_id_type=MESH)
        return carry

    lax.fori_loop(1, ntp, one, 0)
    pl.semaphore_signal(barrier, inc=1, device_id={"z": (z + 1) % nz}, device_id_type=MESH)
    pl.semaphore_signal(barrier, inc=1, device_id={"z": (z + nz - 1) % nz}, device_id_type=MESH)
    pl.semaphore_signal(barrier, inc=1, device_id={"c": 1 - c}, device_id_type=MESH)
    pl.semaphore_wait(barrier, ntp - 1 + 3)


def wait_bytes(ref, sem):
    pltpu.make_async_copy(ref, ref, sem).wait()


class Ring:
    def __init__(self, buf, z, c, nz, send_sem, recv_sem, pair_sem):
        self.buf, self.z, self.c, self.nz = buf, z, c, nz
        self.h = nz // 2
        self.send_sem, self.recv_sem, self.pair_sem = send_sem, recv_sem, pair_sem

    def piece(self, chip, core, sub):
        return self.buf.at[chip * 2 + core, pl.ds(sub * HALF, HALF)]

    def hop(self, chip, direction, sub, step):
        to = (self.z + (1 if direction == 0 else self.nz - 1)) % self.nz
        part = self.piece(chip, self.c, sub)
        return pltpu.make_async_remote_copy(
            src_ref=part,
            dst_ref=part,
            send_sem=self.send_sem,
            recv_sem=self.recv_sem.at[direction, sub, step],
            device_id={"z": to},
            device_id_type=MESH,
        )

    def pair(self, chip, sub, order):
        part = self.piece(chip, self.c, sub)
        return pltpu.make_async_remote_copy(
            src_ref=part,
            dst_ref=part,
            send_sem=self.send_sem,
            recv_sem=self.pair_sem.at[order, sub],
            device_id={"c": 1 - self.c},
            device_id_type=MESH,
        )

    def begin(self):
        for sub in range(2):
            for direction in range(2):
                self.hop(self.z, direction, sub, 1).start()
        for sub in range(2):
            self.pair(self.z, sub, 0).start()

    def step(self, s):
        h, nz = self.h, self.nz
        for sub in range(2):
            for direction in range(2):
                chip = (self.z + (nz - s if direction == 0 else s)) % nz
                order = jnp.minimum(2 * s - 1 + direction, 2 * h - 1)
                last = h if direction == sub else h - 1

                @pl.when(s <= last)
                def _():
                    wait_bytes(self.piece(chip, self.c, sub), self.recv_sem.at[direction, sub, s])

                @pl.when(s < last)
                def _():
                    self.hop(chip, direction, sub, s + 1).start()

                @pl.when(s <= last)
                def _():
                    self.pair(chip, sub, order).start()

    def wait_pair(self, chip, order):
        for sub in range(2):
            wait_bytes(self.piece(chip, 1 - self.c, sub), self.pair_sem.at[order, sub])

    def finish(self):
        wait_bytes(self.buf.at[pl.ds(0, 2 * self.nz - 1)], self.send_sem)


def attention_kernel(
    dims,
    q_ref, k_ref, v_ref, qg_ref, kg_ref, res_ref, ow_ref, route_ref, rowtab_ref, coltab_ref,
    mixed_ref, routes_ref,
    kvbuf, rbuf, qz, run_max, run_sum, acc, attsend, attbuf,
    ring_send, ring_recv, ring_pair, route_send, route_recv, route_pair, att_send, att_recv,
):
    nz, ny, nx = dims
    ntp = ny * nx
    h = nz // 2
    z, c, y, x = places()
    me = y * nx + x
    sp = z * 2 + c
    ring = Ring(kvbuf, z, c, nz, ring_send, ring_recv, ring_pair)

    lane = lax.broadcasted_iota(jnp.int32, (64, LANES), 1)
    low = lane < 64
    even = (lane // 16) % 2 == 0
    row_half = (lane % 64) < 32

    def normed(values, gain, both):
        squares = values * values
        first = jnp.sum(jnp.where(low, squares, 0.0), axis=1, keepdims=True) / 64.0
        scale = lax.rsqrt(first + EPS)
        if both:
            second = jnp.sum(jnp.where(low, 0.0, squares), axis=1, keepdims=True) / 64.0
            scale = jnp.where(low, scale, lax.rsqrt(second + EPS))
        return values * scale * gain

    def turned(values, cosine, sine):
        partner = jnp.where(even, pltpu.roll(values, 112, 1), pltpu.roll(values, 16, 1))
        return values * cosine + partner * sine

    kgain = jnp.concatenate([kg_ref[...], kg_ref[...]], axis=1)
    qgain = jnp.concatenate([qg_ref[0:1, :], qg_ref[1:2, :]], axis=1)
    for part in range(4):
        rows = slice(part * 64, part * 64 + 64)
        row = sp * 4 + part
        cosine = jnp.where(row_half, rowtab_ref[0, pl.ds(row, 1), :], coltab_ref[0])
        sine = jnp.where(row_half, rowtab_ref[1, pl.ds(row, 1), :], coltab_ref[1])
        packed = jnp.concatenate([k_ref[rows, :], v_ref[rows, :]], axis=1).astype(F32)
        keys = turned(normed(packed, kgain, False), cosine, sine)
        kvbuf[sp, rows, :] = jnp.where(low, keys, packed).astype(BF16)
        query = turned(normed(q_ref[rows, :].astype(F32), qgain, True), cosine, sine)
        query = query.astype(BF16).astype(F32) * 0.125
        qz[rows, :] = jnp.where(low, query, 0.0).astype(BF16)
        qz[slice(TOK + part * 64, TOK + part * 64 + 64), :] = jnp.where(
            low, pltpu.roll(query, 64, 1), 0.0
        ).astype(BF16)
    rbuf[sp] = route_ref[...]
    run_max[...] = jnp.full((1, 2 * TOK), -1e30, F32)
    run_sum[...] = jnp.zeros((1, 2 * TOK), F32)
    acc[...] = jnp.zeros((LANES, 2 * TOK), F32)

    barrier_all(z, c, me, nz, ntp, nx)
    ring.begin()

    def route_hop(chip, direction, step):
        to = (z + (1 if direction == 0 else nz - 1)) % nz
        part = rbuf.at[chip * 2 + c]
        return pltpu.make_async_remote_copy(
            src_ref=part, dst_ref=part, send_sem=route_send,
            recv_sem=route_recv.at[direction, step],
            device_id={"z": to}, device_id_type=MESH,
        )

    def route_cross(chip, order):
        part = rbuf.at[chip * 2 + c]
        return pltpu.make_async_remote_copy(
            src_ref=part, dst_ref=part, send_sem=route_send,
            recv_sem=route_pair.at[order],
            device_id={"c": 1 - c}, device_id_type=MESH,
        )

    for direction in range(2):
        route_hop(z, direction, 1).start()
    route_cross(z, 0).start()

    def update(u, carry):
        g = (u + 1) // 2
        chip = (z + nz + (1 - 2 * (u % 2)) * g) % nz
        ring.wait_pair(chip, u)
        block = kvbuf[pl.ds(chip * 2, 2)].reshape(2 * TOK, LANES)
        scores = lax.dot_general(
            block, qz[...], (((1,), (1,)), ((), ())), preferred_element_type=F32
        )
        old = run_max[...]
        new = jnp.maximum(old, jnp.max(scores, axis=0, keepdims=True))
        weights = jnp.exp(scores - new).astype(BF16)
        rescale = jnp.exp(old - new)
        run_max[...] = new
        run_sum[...] = run_sum[...] * rescale + jnp.sum(
            weights.astype(F32), axis=0, keepdims=True
        )
        acc[...] = acc[...] * rescale + lax.dot_general(
            block, weights, (((0,), (0,)), ((), ())), preferred_element_type=F32
        )
        return carry

    def step(s, carry):
        @pl.when(s <= h)
        def _():
            ring.step(s)
            for direction in range(2):
                chip = (z + (nz - s if direction == 0 else s)) % nz
                last = h - direction

                @pl.when(s <= last)
                def _():
                    wait_bytes(rbuf.at[chip * 2 + c], route_recv.at[direction, s])

                @pl.when(s < last)
                def _():
                    route_hop(chip, direction, s + 1).start()

                @pl.when(s <= last)
                def _():
                    route_cross(chip, 2 * s - 1 + direction).start()

        lax.fori_loop(jnp.maximum(2 * s - 3, 0), jnp.minimum(2 * s - 1, 2 * h), update, 0)
        return carry

    lax.fori_loop(1, h + 2, step, 0)

    value = acc[64:128, :] / run_sum[...]
    stacked = jnp.concatenate([value[:, 0:TOK], value[:, TOK : 2 * TOK]], axis=0)
    attended = stacked.T.astype(BF16)
    attsend[...] = attended
    mine = pl.ds(pl.multiple_of(me * LANES, LANES), LANES)
    attbuf[:, mine] = attended

    def spread(d, carry):
        t = (me + d) % ntp
        pltpu.make_async_remote_copy(
            src_ref=attsend, dst_ref=attbuf.at[:, mine], send_sem=att_send, recv_sem=att_recv,
            device_id=plane_id(t, nx), device_id_type=MESH,
        ).start()
        return carry

    lax.fori_loop(1, ntp, spread, 0)

    def route_wait(u, carry):
        g = (u + 1) // 2
        chip = (z + nz + (1 - 2 * (u % 2)) * g) % nz
        wait_bytes(rbuf.at[chip * 2 + 1 - c], route_pair.at[u])
        return carry

    lax.fori_loop(0, 2 * h, route_wait, 0)
    routes_ref[...] = rbuf[...]
    ring.finish()
    wait_bytes(rbuf.at[pl.ds(0, 2 * nz - 1)], route_send)
    pieces = kvbuf.at[pl.ds(0, ntp - 1)]
    wait_bytes(pieces, att_recv)
    mixed_ref[...] = res_ref[...].astype(F32) + jnp.dot(
        attbuf[...], ow_ref[...], preferred_element_type=F32
    )
    wait_bytes(pieces, att_send)


def expert_kernel(
    dims,
    mixed_ref, routes_ref, gate_ref, up_ref, down_ref,
    out_ref,
    rowbuf, marks, keyb, wb, sbuf, wrow, sendd, xbuf, wg, wu, wd, rsend, ret,
    keep, psend, prs, rss, rsr,
    ring_send, ring_recv, ring_pair, disp_send, disp_recv, disp_own, weight_sem,
    ret_send, ret_recv, ret_own, pair_send, pair_recv, rs_send, rs_recv,
):
    nz, ny, nx = dims
    ntp = ny * nx
    h = nz // 2
    experts = ntp // 2
    width = ntp * LANES
    z, c, y, x = places()
    me = y * nx + x
    sp = z * 2 + c
    column, half = me // 2, me % 2
    ring = Ring(rowbuf, z, c, nz, ring_send, ring_recv, ring_pair)

    rowbuf[sp] = mixed_ref[...].astype(BF16)
    loads = [
        pltpu.make_async_copy(source.at[0], target, weight_sem.at[i])
        for i, (source, target) in enumerate(((gate_ref, wg), (up_ref, wu), (down_ref, wd)))
    ]
    for load in loads:
        load.start()
    barrier_all(z, c, me, nz, ntp, nx)
    ring.begin()

    number = (sp * experts + lax.broadcasted_iota(jnp.int32, (8, TOK), 0)).astype(F32)

    def mark(b, carry):
        hit = jnp.zeros((8, TOK), F32)
        weight = jnp.zeros((8, TOK), F32)
        for k in range(8):
            same = routes_ref[b, k : k + 1, :] == number
            hit = hit + jnp.where(same, 1.0, 0.0)
            weight = weight + jnp.where(same, routes_ref[b, 8 + k : 9 + k, :], 0.0)
        marks[b] = hit
        wb[b] = weight
        return carry

    lax.fori_loop(0, 2 * nz, mark, 0)
    before = jnp.where(
        lax.broadcasted_iota(jnp.int32, (TOK, TOK), 0)
        < lax.broadcasted_iota(jnp.int32, (TOK, TOK), 1),
        1.0,
        0.0,
    ).astype(BF16)
    flat = marks[...].reshape(2 * nz * 8, TOK)
    rank = jnp.dot(flat.astype(BF16), before, preferred_element_type=F32)
    keyb[...] = jnp.where(flat > 0.5, rank, -1000.0).reshape(2 * nz, 8, TOK)
    slot = lax.broadcasted_iota(jnp.int32, (GROUP, TOK), 0).astype(F32)

    def chips(g):
        return (z + nz - g) % nz, (z + g % h) % nz

    def dispatch(g):
        first, second = chips(g)
        ring.wait_pair(first, 2 * g - 1)
        ring.wait_pair(second, 2 * g % (2 * h))
        total = jnp.zeros((GROUP, TOK), F32)
        for i in range(4):
            b = (first if i < 2 else second) * 2 + i % 2
            key = keyb[b]
            for j in range(experts):
                hit = key[j : j + 1, :] + float(CAP * i) == slot
                sbuf[g - 1, j * GROUP : (j + 1) * GROUP, i * TOK : (i + 1) * TOK] = jnp.where(
                    hit, 1.0, 0.0
                ).astype(BF16)
            own_key = keyb[b, pl.ds(column, 1), :]
            own_weight = wb[b, pl.ds(column, 1), :]
            total = total + jnp.where(own_key + float(CAP * i) == slot, own_weight, 0.0)
        wrow[g - 1] = jnp.broadcast_to(jnp.sum(total, axis=1, keepdims=True), (GROUP, LANES))
        chosen = jnp.dot(
            sbuf[g - 1, :, 0 : 2 * TOK],
            rowbuf[pl.ds(first * 2, 2)].reshape(2 * TOK, LANES),
            preferred_element_type=F32,
        ) + jnp.dot(
            sbuf[g - 1, :, 2 * TOK : 4 * TOK],
            rowbuf[pl.ds(second * 2, 2)].reshape(2 * TOK, LANES),
            preferred_element_type=F32,
        )
        sendd[g - 1] = chosen.astype(BF16).reshape(experts, GROUP, LANES)
        target = xbuf.at[
            pl.ds(pl.multiple_of((g - 1) * GROUP, 16), GROUP),
            pl.ds(pl.multiple_of(me * LANES, LANES), LANES),
        ]

        def one(d, carry):
            t = (me + d) % ntp
            pltpu.make_async_remote_copy(
                src_ref=sendd.at[g - 1, t // 2], dst_ref=target,
                send_sem=disp_send, recv_sem=disp_recv.at[g - 1],
                device_id=plane_id(t, nx), device_id_type=MESH,
            ).start()
            return carry

        lax.fori_loop(1, ntp, one, 0)
        pltpu.make_async_copy(sendd.at[g - 1, column], target, disp_own.at[g - 1]).start()

    pieces = ret.at[pl.ds(0, ntp - 1)]

    def compute(p):
        for k in range(2):
            wait_bytes(pieces, disp_recv.at[2 * p + k])
            wait_bytes(ret.at[0], disp_own.at[2 * p + k])
        rows = xbuf[pl.ds(pl.multiple_of(p * 2 * GROUP, 16), 2 * GROUP), :]
        wide = rows.astype(F32)
        scale = lax.rsqrt(jnp.sum(wide * wide, axis=1, keepdims=True) / float(width) + EPS)
        gate = jnp.dot(rows, wg[...], preferred_element_type=F32) * scale
        up = jnp.dot(rows, wu[...], preferred_element_type=F32) * scale
        hidden = (gate / (1.0 + jnp.exp(-gate)) * up).astype(BF16)
        factor = wrow[pl.ds(2 * p, 2)].reshape(2 * GROUP, LANES)

        def slices(n, carry):
            columns = pl.ds(pl.multiple_of(n * 2 * LANES, 2 * LANES), 2 * LANES)
            result = jnp.dot(hidden, wd[:, columns], preferred_element_type=F32)
            result = result.astype(BF16).astype(F32)
            for k in range(2):
                part = result[:, k * LANES : (k + 1) * LANES] * factor
                rsend[2 * n + k, pl.ds(2 * p, 2)] = part.astype(BF16).reshape(2, GROUP, LANES)
            return carry

        lax.fori_loop(0, ntp // 2, slices, 0)

    early = max(0, (h - 5) // 2 + 1)
    chunks = h // 2

    def step(s, carry):
        @pl.when(s <= h)
        def _():
            ring.step(s)

        @pl.when((s >= 2) & (s <= h + 1))
        def _():
            dispatch(s - 1)

        @pl.when(s == min(5, h + 2))
        def _():
            for load in loads:
                load.wait()

        is_early = (s >= 5) & (s <= h) & ((s + 1) % 2 == 0)

        @pl.when(is_early | (s >= h + 2))
        def _():
            compute(jnp.where(s >= h + 2, early + s - (h + 2), (s - 5) // 2))

        return carry

    lax.fori_loop(1, h + 2 + chunks - early, step, 0)

    def give(i, carry):
        g = h - i
        target = ret.at[(g - 1) * ntp + half * experts + column]

        def one(d, inner):
            t = (me + d) % ntp
            pltpu.make_async_remote_copy(
                src_ref=rsend.at[t, g - 1], dst_ref=target,
                send_sem=ret_send, recv_sem=ret_recv.at[g - 1],
                device_id=plane_id(t, nx), device_id_type=MESH,
            ).start()
            return inner

        lax.fori_loop(1, ntp, one, 0)
        pltpu.make_async_copy(rsend.at[me, g - 1], target, ret_own.at[g - 1]).start()
        return carry

    lax.fori_loop(0, h, give, 0)

    def combine(g):
        wait_bytes(pieces, ret_recv.at[g - 1])
        wait_bytes(ret.at[0], ret_own.at[g - 1])
        blocks = [
            ret[pl.ds((g - 1) * ntp + k * experts, experts)].reshape(experts * GROUP, LANES)
            for k in range(2)
        ]

        def partial(side, core):
            columns = pl.ds(pl.multiple_of(side * 2 * TOK + core * TOK, TOK), TOK)
            chosen = sbuf[g - 1, :, columns]
            return lax.dot_general(
                chosen, blocks[0], (((0,), (0,)), ((), ())), preferred_element_type=F32
            ) + lax.dot_general(
                chosen, blocks[1], (((0,), (0,)), ((), ())), preferred_element_type=F32
            )

        for side in range(2):
            psend[(g - 1) * 2 + side] = partial(side, 1 - c).astype(BF16)
            pltpu.make_async_remote_copy(
                src_ref=psend.at[(g - 1) * 2 + side], dst_ref=prs.at[(g - 1) * 2 + side],
                send_sem=pair_send, recv_sem=pair_recv.at[(g - 1) * 2 + side],
                device_id={"c": 1 - c}, device_id_type=MESH,
            ).start()
        for side in range(2):
            keep[(g - 1) * 2 + side] = partial(side, c)

    def pass_on(r):
        g = h + 1 - r
        for side in range(2):
            wait_bytes(prs.at[(g - 1) * 2 + side], pair_recv.at[(g - 1) * 2 + side])
        for sub in range(2):
            rows = slice(sub * HALF, sub * HALF + HALF)
            for direction in range(2):
                index = (g - 1) * 2 + jnp.where(r == 1, 0, 1 - direction)
                same = direction == sub
                first_send = 1 if same else 2
                first_add = 2 if same else 3
                slot_of = (direction * 2 + sub) * h + r - 1

                @pl.when(r >= first_add)
                def _():
                    wait_bytes(rsr.at[slot_of - 1], rs_recv.at[slot_of - 1])
                    rss[slot_of] = (
                        keep[index, rows, :]
                        + prs[index, rows, :].astype(F32)
                        + rsr[slot_of - 1].astype(F32)
                    ).astype(BF16)

                @pl.when(r == first_send)
                def _():
                    rss[slot_of] = (
                        keep[index, rows, :] + prs[index, rows, :].astype(F32)
                    ).astype(BF16)

                @pl.when(r >= first_send)
                def _():
                    to = (z + (1 if direction == 0 else nz - 1)) % nz
                    pltpu.make_async_remote_copy(
                        src_ref=rss.at[slot_of], dst_ref=rsr.at[slot_of],
                        send_sem=rs_send, recv_sem=rs_recv.at[slot_of],
                        device_id={"z": to}, device_id_type=MESH,
                    ).start()

    def back(s, carry):
        @pl.when(s <= h)
        def _():
            combine(h + 1 - s)

        @pl.when(s >= 2)
        def _():
            pass_on(s - 1)

        return carry

    lax.fori_loop(1, h + 2, back, 0)

    own = (h - 1) * 2 + 1
    for sub in range(2):
        rows = slice(sub * HALF, sub * HALF + HALF)
        total = mixed_ref[rows, :] + keep[own, rows, :] + prs[own, rows, :].astype(F32)
        for direction in range(2):
            slot_of = (direction * 2 + sub) * h + h - 1
            wait_bytes(rsr.at[slot_of], rs_recv.at[slot_of])
            total = total + rsr[slot_of].astype(F32)
        out_ref[rows, :] = total.astype(BF16)

    ring.finish()
    wait_bytes(ret.at[pl.ds(0, h * (ntp - 1))], disp_send)
    wait_bytes(ret.at[pl.ds(0, h * (ntp - 1))], ret_send)
    wait_bytes(prs, pair_send)
    wait_bytes(rsr.at[pl.ds(0, 4 * h - 2)], rs_send)


def local(dims, q, k, v, q_gain, k_gain, residual, out_weight, route_expert, route_weight, gate, up, down):
    nz, ny, nx = dims
    ntp = ny * nx
    h = nz // 2
    width = ntp * LANES
    experts = ntp // 2
    vmem = pl.BlockSpec(memory_space=pltpu.VMEM)
    hbm = pl.BlockSpec(memory_space=pl.ANY)
    dma = pltpu.SemaphoreType.DMA
    route = jnp.concatenate([route_expert.astype(F32).T, route_weight.T], axis=0)
    rowtab, coltab = rotation_constants(nz * 8)
    mixed, routes = pl.pallas_call(
        functools.partial(attention_kernel, dims),
        out_shape=(
            jax.ShapeDtypeStruct((TOK, LANES), F32),
            jax.ShapeDtypeStruct((2 * nz, 16, TOK), F32),
        ),
        in_specs=[vmem] * 10,
        out_specs=(vmem, vmem),
        scratch_shapes=[
            pltpu.VMEM((2 * nz, TOK, LANES), BF16),
            pltpu.VMEM((2 * nz, 16, TOK), F32),
            pltpu.VMEM((2 * TOK, LANES), BF16),
            pltpu.VMEM((1, 2 * TOK), F32),
            pltpu.VMEM((1, 2 * TOK), F32),
            pltpu.VMEM((LANES, 2 * TOK), F32),
            pltpu.VMEM((TOK, LANES), BF16),
            pltpu.VMEM((TOK, width), BF16),
            dma, dma((2, 2, h + 1)), dma((2 * h, 2)),
            dma, dma((2, h + 1)), dma((2 * h,)),
            dma, dma,
        ],
        compiler_params=pltpu.CompilerParams(
            collective_id=0, has_side_effects=True, vmem_limit_bytes=40 * 1024 * 1024
        ),
        name="attend",
    )(q, k, v, q_gain, k_gain, residual, out_weight, route, jnp.asarray(rowtab), jnp.asarray(coltab))
    rows = h * GROUP
    return pl.pallas_call(
        functools.partial(expert_kernel, dims),
        out_shape=jax.ShapeDtypeStruct((TOK, LANES), BF16),
        in_specs=[vmem, vmem, hbm, hbm, hbm],
        out_specs=vmem,
        scratch_shapes=[
            pltpu.VMEM((2 * nz, TOK, LANES), BF16),
            pltpu.VMEM((2 * nz, 8, TOK), F32),
            pltpu.VMEM((2 * nz, 8, TOK), F32),
            pltpu.VMEM((2 * nz, 8, TOK), F32),
            pltpu.VMEM((h, experts * GROUP, 4 * TOK), BF16),
            pltpu.VMEM((h, GROUP, LANES), F32),
            pltpu.VMEM((h, experts, GROUP, LANES), BF16),
            pltpu.VMEM((rows, width), BF16),
            pltpu.VMEM((width, 256), BF16),
            pltpu.VMEM((width, 256), BF16),
            pltpu.VMEM((256, width), BF16),
            pltpu.VMEM((ntp, h, GROUP, LANES), BF16),
            pltpu.VMEM((h * ntp, GROUP, LANES), BF16),
            pltpu.VMEM((2 * h, TOK, LANES), F32),
            pltpu.VMEM((2 * h, TOK, LANES), BF16),
            pltpu.VMEM((2 * h, TOK, LANES), BF16),
            pltpu.VMEM((4 * h, HALF, LANES), BF16),
            pltpu.VMEM((4 * h, HALF, LANES), BF16),
            dma, dma((2, 2, h + 1)), dma((2 * h, 2)),
            dma, dma((h,)), dma((h,)), dma((3,)),
            dma, dma((h,)), dma((h,)),
            dma, dma((2 * h,)), dma, dma((4 * h,)),
        ],
        compiler_params=pltpu.CompilerParams(
            collective_id=1, has_side_effects=True, vmem_limit_bytes=60 * 1024 * 1024
        ),
        name="experts",
    )(mixed, routes, gate, up, down)


def build(devices, dims):
    nz, ny, nx = dims
    split = Mesh(devices.reshape(nz, 2, ny, nx), ALL)
    in_specs = (
        P(SP, TP), P(SP, TP), P(SP, TP), P(TP, None), P(TP, None), P(SP, TP), P(None, TP),
        P(SP, None), P(SP, None), P(ALL, None, None), P(ALL, None, None), P(ALL, None, None),
    )
    return jax.shard_map(
        functools.partial(local, dims), mesh=split, in_specs=in_specs,
        out_specs=P(SP, TP), check_vma=False,
    )


def solution(mesh):
    return build(mesh.devices, (mesh.shape["sp"] // 2, 4, mesh.shape["tp"] // 4))
```

time: 402 us -> 151 us (0.38)
  waiting for transfers between devices: 170 us -> 0 us
  Pallas kernels: 0 us -> 139 us
  blocking collectives: 75.7 us -> 0 us
  local copies, waits for them, and re-layouts: 61.2 us -> 7.42 us
  matrix products: 30.6 us -> 0 us
  starting transfers between devices: 24.4 us -> 0 us
  other arithmetic: 19.1 us -> 1.43 us
  between operations: 13.9 us -> 0.1 us
    pallas_call x0 -> x2, Pallas kernels: none -> 139 us  [the longest x1 80 us: local(): pl.pallas_call(functools.partial(expert_kernel, dims), out_shape=jax.Shap...]
    all_to_all x3 -> x0, waiting for transfers between devices: 82.4 us -> none  [the longest x1 61.6 us: turned_blocks(): lax.all_to_all(pieces, axes[k], split_axis=k, concat_axis=k, tiled=True)]
    all_to_all x4 -> x0, blocking collectives: 75.7 us -> none  [the longest x3 61.1 us: turned_blocks(): lax.all_to_all(pieces, axes[k], split_axis=k, concat_axis=k, tiled=True)]
    all_gather x1 -> x0, waiting for transfers between devices: 75.3 us -> none  [local(): incoming = lax.all_gather(packed, SP, axis=0, tiled=True)]
    dot_general x19 -> x0, matrix products: 30.6 us -> none  [the longest x8 11.1 us: online_update(): jnp.einsum('kgtn,nkd->kgtd', weights, value_block, preferred_element_type...]
    all_to_all x3 -> x0, starting transfers between devices: 22.3 us -> none  [the longest x1 11.2 us: turned_blocks(): lax.all_to_all(pieces, axes[k], split_axis=k, concat_axis=k, tiled=True)]
    gather x9 -> x0, local copies, waits for them, and re-layouts: 22 us -> none  [the longest x8 18.8 us: local(): picked = slot_results[index].astype(jnp.float32)]
    ppermute x1 -> x0, waiting for transfers between devices: 12.4 us -> none  [swapped(): return lax.ppermute(value, axis, pairs)]
  transfers between devices with their start and end apart: 5 -> 0, of which waited for: 5 -> 0; matrix products, arithmetic and copies ran while one was open for 5% -> 0% of each run, Pallas kernels for 0% -> 0%
where the time goes in v1:
time: 151 us; the launch traced here: 148 us
  Pallas kernels  139 us (92%)
  local copies, waits for them, and re-layouts  7.42 us (5%)
    pallas_call x1, Pallas kernels, local(): pl.pallas_call(functools.partial(expert_kernel, dims), out_shape=jax.Shap...  80 us
    pallas_call x1, Pallas kernels, local(): pl.pallas_call(functools.partial(attention_kernel, dims), out_shape=(jax....  59.5 us
    unnamed x21, local copies, waits for them, and re-layouts  7.42 us

profile of v1, /device:TPU:1, one launch (start us, length us, event | category | flops | bytes accessed | tf_op | source)
XLA Modules:
  0.0 148.4 jit_solution(2721058779009102421)
XLA Ops:
  0.0 0.0 copy-start.2
  0.0 0.7 convert_bitcast_fusion
  0.7 0.7 pad_maximum_fusion.route_ref
  1.4 0.9 copy.15.k_ref
  2.3 0.0 copy-start.4
  2.3 0.0 copy-start.7
  2.3 0.0 copy-start.8
  2.3 0.9 copy.16.v_ref
  3.3 0.0 copy-done.2
  3.3 0.0 copy-done.4
  3.3 0.0 copy-done.7
  3.3 0.0 copy-done.8
  3.3 0.0 copy-start
  3.3 1.0 copy-done
  4.3 0.0 copy-start.5
  4.3 0.8 copy-done.5
  5.2 0.0 copy-start.6
  5.2 0.8 copy-done.6
  6.0 59.5 %attend.1 = (f32[256,128]{1,0:T(8,128)S(1)}, f32[32,16,256]{2,1,0:T(8,128)S(1)}) custom-call(bf16[256,128]{1,0:T(8,128)(2,1)S(1)} %copy-done.4, bf16[256,64]{1,0:T(8,128)(2,1)S(1)} %copy.15.k_ref, bf16[256,64]{1,0:T(8,128)(2,1)S(1)} %copy.16.v_ref, f32[2,64]{1,0:T(2,128)S(1)} %copy-done.7, f32[1,64]{1,0:T(1,128)S(1)} %copy-done.8, ...), custom_call_target="tpu_custom_call" | custom-call | tf_op jit(solution)/shard_map/attend/pallas_call | solution.py:573
  65.5 0.0 copy-start.1
  65.5 0.8 copy-done.1
  66.3 0.6 copy-done.3
  67.0 80.0 %experts.1 = bf16[256,128]{1,0:T(8,128)(2,1)} custom-call(f32[256,128]{1,0:T(8,128)} %copy-done.3, f32[32,16,256]{2,1,0:T(8,128)} %copy-done.1, bf16[1,2048,256]{2,1,0:T(8,128)(2,1)} %gate_ref.1, bf16[1,2048,256]{2,1,0:T(8,128)(2,1)} %up_ref.1, bf16[1,256,2048]{2,1,0:T(8,128)(2,1)} %down_ref.1), custom_call_target="tpu_custom_call" | custom-call | tf_op jit(solution)/shard_map/experts/pallas_call | solution.py:600
  146.9 1.5 copy.18
  (1 shorter events, 0.0 us)
Async XLA Ops:
  0.0 3.3 %copy-start.2 = (f32[2,128,128]{2,1,0:T(8,128)S(1)}, f32[2,128,128]{2,1,0:T(8,128)}, u32[]{:S(2)}) copy-start(f32[2,128,128]{2,1,0:T(8,128)} %constant.4.clone.rowtab_ref) | copy-start | bytes 393220
  2.3 1.0 copy-start.4
  2.3 1.0 copy-start.7
  2.3 0.9 copy-start.8
  3.3 1.0 copy-start
  4.3 0.8 copy-start.5
  5.2 0.8 copy-start.6
  65.5 0.8 copy-start.1
  66.3 0.6 copy-start.3
